TPU v7x, 32 devices: a whole 2x2x4 slice. The times are simulated.
32 devices in a mesh: sp: 4 (over z), dp: 8 (over y, x, core).
Axes of the slice: x: 2, y: 2, z: 4, core: 2. Of those that a mesh axis runs over, the one named last changes fastest.
Arguments:
- hidden: bfloat16 [8, 512, 2048], P('dp', 'sp'), may hold values from -6 to 6
- queries: bfloat16 [8, 512, 1024], P('dp', 'sp'), may hold values from -6 to 6
- values: bfloat16 [8, 512, 2048], P('dp', 'sp'), may hold values from -6 to 6
- key_weight: bfloat16 [2048, 1024], P('dp'), may hold values from -0.125 to 0.125
- decay_down: bfloat16 [2048, 16], replicated, may hold values from -0.125 to 0.125
- decay_up: float32 [16, 1024], replicated, may hold values from -1.5 to 1.5
- decay_bias: float32 [1024], replicated, may hold values from -1 to 8
- span_shift: bfloat16 [8, 512], P('dp', 'sp'), may hold values from -1.5 to 1.5, as said below
- norm_gain: float32 [2048], replicated, may hold values from 0.1 to 1.9
Outputs:
- attended: bfloat16 [8, 512, 2048], P('dp', 'sp')
Inputs may be any that keep to these rules, and one draw needn't show every extreme that they name: `span_shift`: constant over each aligned block of 64 positions.
All inputs are finite; a program needn't handle non-finite values.
Results may differ from a plain program's by a relative error of at most 0.0073.
Values may be sent and summed in bfloat16 or wider, within the bound.
A program may use at most 64 MiB of HBM per device.

v0:
```python
import functools

import jax
import jax.numpy as jnp
from jax import lax
from jax.experimental import pallas as pl
from jax.experimental.pallas import tpu as pltpu
from jax.sharding import PartitionSpec as P

HEADS = 4
DK = 256
DV = 512
BLOCK = 64
KEY = 1024
VAL = 2048
CORES = 2
SPLIT = 4
DVS = DV // SPLIT

decay_tau = 16.0
norm_eps = 1e-05
highest = lax.Precision.HIGHEST
MESH = pl.DeviceIdType.MESH
f32 = jnp.float32
bf16 = jnp.bfloat16


def each(low, high, fn):
    if high - low <= 4:
        for j in range(low, high):
            fn(j)
    else:
        lax.fori_loop(low, high, lambda j, c: (fn(j), c)[1], 0)


def dot_nt(a, b):
    return lax.dot_general(a, b, (((1,), (1,)), ((), ())), preferred_element_type=f32)


def dot_tn(a, b):
    return lax.dot_general(a, b, (((0,), (0,)), ((), ())), preferred_element_type=f32)


def kernel(
    n_sp, n_dp,
    hid, que, val, kw, down, up, bias, shift, gain,
    out,
    wbuf, hv, qv, vv, outv, qf, qb, qx, qs, fac, rate, local, sbuf, rbuf, acc,
    lsem, osem, wsend, wrecv, psend, precv, csend, crecv, dsend, drecv,
):
    sp = lax.axis_index("sp")
    dp = lax.axis_index("dp")
    chips = n_dp // CORES
    chip = dp // CORES
    core = dp % CORES
    partner = chip * CORES + (1 - core)
    tok = hv.shape[0]
    depth = kw.shape[0]

    square = chips == 4
    half = depth // 2

    def across(j):
        return (chip + 1 - 2 * lax.rem(chip, 2), lax.rem(chip + 2, 4), 3 - chip)[j - 1]

    def peer(j):
        if square:
            return across(j) * CORES + core
        return lax.rem(chip + j, chips) * CORES + core

    def source_chip(j):
        if square:
            return chip if j == 0 else across(j)
        return lax.rem(chip - j + chips, chips)

    wlocal = [
        pltpu.make_async_copy(kw.at[:, pl.ds(h * DK, DK)], wbuf.at[h, dp], lsem.at[h])
        for h in range(HEADS)
    ]
    inputs = [
        pltpu.make_async_copy(a, b, lsem.at[HEADS + i])
        for i, (a, b) in enumerate(((hid, hv), (que, qv), (val, vv)))
    ]
    for c in wlocal + inputs:
        c.start()

    barrier = pltpu.get_barrier_semaphore()
    each(1, chips, lambda j: pl.semaphore_signal(
        barrier, inc=1, device_id={"dp": peer(j)}, device_id_type=MESH))
    pl.semaphore_signal(barrier, inc=1, device_id={"dp": partner}, device_id_type=MESH)

    for side in (1, n_sp - 1):
        pl.semaphore_signal(
            barrier, inc=1, device_id={"sp": lax.rem(sp + side, n_sp)}, device_id_type=MESH)
    pl.semaphore_wait(barrier, chips + 2)

    def wcopy(h, j):
        return pltpu.make_async_remote_copy(
            src_ref=wbuf.at[h, dp], dst_ref=wbuf.at[h, dp],
            send_sem=wsend.at[h, j], recv_sem=wrecv.at[h, j],
            device_id={"dp": peer(j)}, device_id_type=MESH)

    def wland(h, j):
        slot = wbuf.at[h, source_chip(j) * CORES + core]
        return pltpu.make_async_remote_copy(
            src_ref=slot, dst_ref=slot,
            send_sem=wsend.at[h, j], recv_sem=wrecv.at[h, j],
            device_id={"dp": peer(j)}, device_id_type=MESH)

    def pcopy(h, j):
        slot = wbuf.at[h, source_chip(j) * CORES + core]
        return pltpu.make_async_remote_copy(
            src_ref=slot, dst_ref=slot,
            send_sem=psend.at[h, j], recv_sem=precv.at[h, j],
            device_id={"dp": partner}, device_id_type=MESH)

    def pland(h, j):
        slot = wbuf.at[h, source_chip(j) * CORES + (1 - core)]
        return pltpu.make_async_remote_copy(
            src_ref=slot, dst_ref=slot,
            send_sem=psend.at[h, j], recv_sem=precv.at[h, j],
            device_id={"dp": partner}, device_id_type=MESH)

    direct = 3 if square else chips

    def diagonal(h, i, lands):
        origin = source_chip(3) if lands else source_chip(1 + i)
        slot = wbuf.at[h, origin * CORES + core, pl.ds(i * half, half), :]
        return pltpu.make_async_remote_copy(
            src_ref=slot, dst_ref=slot,
            send_sem=dsend.at[h, i], recv_sem=drecv.at[h, i],
            device_id={"dp": peer(2 - i)}, device_id_type=MESH)

    def phase_send(h):
        wlocal[h].wait()
        each(1, direct, lambda j: wcopy(h, j).start())
        pcopy(h, 0).start()

    def phase_relay(h):
        def relay(j):
            wland(h, j).wait_recv()
            if square:
                diagonal(h, j - 1, False).start()
            pcopy(h, j).start()
        each(1, direct, relay)

    ahead = 2 if square else HEADS
    for h in range(ahead):
        phase_send(h)

    inputs[0].wait()
    low = dot_nt(hv[...], down[...]).astype(bf16)
    steps = shift[...].astype(f32)
    inputs[1].wait()
    row = lax.broadcasted_iota(jnp.int32, (tok, DK), 0)
    first = row < BLOCK
    ti = lax.broadcasted_iota(jnp.int32, (tok, tok), 0)
    tj = lax.broadcasted_iota(jnp.int32, (tok, tok), 1)
    same = (ti < BLOCK) == (tj < BLOCK)
    below = tj <= ti
    tri = jnp.where(same & below, 1.0, 0.0).astype(f32)
    def phase_prep(h):
        cols = pl.ds(h * DK, DK)
        pre = jnp.dot(low.astype(f32), up[:, cols], precision=highest, preferred_element_type=f32)
        pre = pre + bias[:, cols] + jnp.where(first, steps[:, :1], steps[:, BLOCK:BLOCK + 1])
        logd = (jnp.minimum(pre, 0.0) - jnp.log1p(jnp.exp(-jnp.abs(pre)))) * (1.0 / decay_tau)
        incl = jnp.dot(tri, logd, precision=highest, preferred_element_type=f32)
        excl = incl - logd
        t0 = incl[BLOCK - 1:BLOCK, :]
        t1 = incl[tok - 1:tok, :]
        here = jnp.where(first, t0, t1)
        after = jnp.where(first, t1, 0.0)
        before = jnp.where(first, 0.0, t0)
        scaled = qv[:, cols].astype(f32) * DK ** (-0.5)
        qf[:, cols] = (scaled * jnp.exp(incl)).astype(bf16)
        qb[:, cols] = (scaled * jnp.exp(-excl)).astype(bf16)
        qx[:, cols] = (scaled * jnp.exp(here - excl)).astype(bf16)
        qs[0, :, cols] = (scaled * jnp.exp(incl + before)).astype(bf16)
        qs[1, :, cols] = (scaled * jnp.exp(here - excl + after)).astype(bf16)
        fac[0, :, cols] = jnp.exp(-incl)
        fac[1, :, cols] = jnp.exp(excl)
        fac[2, :, cols] = jnp.exp(here - incl)
        fac[3, :, cols] = jnp.exp(here - incl + after)
        fac[4, :, cols] = jnp.exp(excl + before)
        rate[:, cols] = jnp.exp(t0 + t1)

    inputs[2].wait()

    def chain(way, h, s):
        target = jnp.clip(sp + 1 - 2 * way, 0, n_sp - 1)
        return pltpu.make_async_remote_copy(
            src_ref=sbuf.at[way, h, s], dst_ref=rbuf.at[way, h, s],
            send_sem=csend.at[way, h, s], recv_sem=crecv.at[way, h, s],
            device_id={"sp": target}, device_id_type=MESH)

    def phase_keys(h):
        if square:
            for i in range(2):
                diagonal(h, i, True).wait_recv()
            pcopy(h, 3).start()
        each(0, chips, lambda j: pland(h, j).wait_recv())
        cols = pl.ds(h * DK, DK)
        weights = wbuf[h].reshape(n_dp * depth, DK)
        keys = jnp.dot(hv[...], weights, preferred_element_type=f32).astype(bf16).astype(f32)
        v = vv[:, pl.ds(h * DV, DV)]
        k_fwd = (keys * fac[3, :, cols]).astype(bf16)
        k_bwd = (keys * fac[4, :, cols]).astype(bf16)
        for way, k in ((0, k_fwd), (1, k_bwd)):
            local[way, h] = dot_tn(v, k)

            @pl.when(sp == (0 if way == 0 else n_sp - 1))
            def _(way=way):
                for s in range(SPLIT):
                    sbuf[way, h, s] = local[way, h, pl.ds(s * DVS, DVS), :].astype(bf16)
                    chain(way, h, s).start()

        kf = (keys * fac[0, :, cols]).astype(bf16)
        kb = (keys * fac[1, :, cols]).astype(bf16)
        ke = (keys * fac[2, :, cols]).astype(bf16)
        query_f, query_b, query_x = qf[:, cols], qb[:, cols], qx[:, cols]
        lower = jnp.where(same, dot_nt(query_f, kf), dot_nt(query_f, ke))
        upper = jnp.where(same, dot_nt(query_b, kb), dot_nt(query_x, kb))
        scores = jnp.where(below, lower, upper).astype(bf16)
        acc[h] = jnp.dot(scores, v, preferred_element_type=f32)

    def phase_chain(way, h):
        cols = pl.ds(h * DK, DK)
        edge = way * (n_sp - 1)
        other = (1 - way) * (n_sp - 1)

        @pl.when(sp != edge)
        def _():
            for s in range(SPLIT):
                rows = pl.ds(s * DVS, DVS)
                chain(way, h, s).wait_recv()

                @pl.when(sp != other)
                def _(s=s, rows=rows):
                    state = rbuf[way, h, s].astype(f32) * rate[:, cols] + local[way, h, rows, :]
                    sbuf[way, h, s] = state.astype(bf16)
                    chain(way, h, s).start()

                acc[h, :, rows] += dot_nt(qs[way, :, cols], rbuf[way, h, s])

    def out_copy(h):
        cols = pl.ds(h * DV, DV)
        return pltpu.make_async_copy(outv.at[:, cols], out.at[:, cols], osem.at[h])

    def phase_out(h):
        cols = pl.ds(h * DV, DV)
        mixed = acc[h].astype(bf16).astype(f32)
        scale = lax.rsqrt(jnp.mean(mixed * mixed, axis=-1, keepdims=True) + norm_eps)
        outv[:, cols] = (mixed * scale * gain[:, cols]).astype(bf16)
        out_copy(h).start()

    near = jnp.where(sp * 2 < n_sp, 0, 1)
    far = 1 - near
    def relay_on(h):
        if h < HEADS:
            phase_relay(h)
            if h + ahead < HEADS:
                phase_send(h + ahead)

    def phase_near(h):
        phase_chain(near, h)

    def phase_far(h):
        phase_chain(far, h)
        phase_out(h)

    plan = ((phase_prep, 0), (relay_on, 0), (phase_prep, 1), (relay_on, 1), (phase_keys, 0), (phase_prep, 2), (relay_on, 2), (phase_keys, 1), (phase_prep, 3), (relay_on, 3), (phase_keys, 2), (phase_near, 0), (phase_keys, 3), (phase_near, 1), (phase_far, 0), (phase_near, 2), (phase_far, 1), (phase_near, 3), (phase_far, 2), (phase_far, 3))
    for phase, h in plan:
        phase(h)

    for h in range(HEADS):
        each(1, direct, lambda j, h=h: wcopy(h, j).wait_send())
        each(0, chips, lambda j, h=h: pcopy(h, j).wait_send())
        if square:
            for i in range(2):
                diagonal(h, i, False).wait_send()
        for way in range(2):
            @pl.when(sp != (1 - way) * (n_sp - 1))
            def _(h=h, way=way):
                for s in range(SPLIT):
                    chain(way, h, s).wait_send()
        out_copy(h).wait()


def body(n_sp, n_dp, hidden, queries, values, key_weight, decay_down, decay_up, decay_bias,
         span_shift, norm_gain):
    seqs, length, width = hidden.shape
    tok = seqs * length
    assert tok == 2 * BLOCK
    chips = n_dp // CORES
    depth = key_weight.shape[0]
    anywhere = pl.BlockSpec(memory_space=pl.ANY)
    vmem = pl.BlockSpec(memory_space=pltpu.VMEM)
    dma = pltpu.SemaphoreType.DMA
    result = pl.pallas_call(
        functools.partial(kernel, n_sp, n_dp),
        out_shape=jax.ShapeDtypeStruct((tok, VAL), bf16),
        in_specs=[anywhere] * 4 + [vmem] * 5,
        out_specs=anywhere,
        scratch_shapes=[
            pltpu.VMEM((HEADS, n_dp, depth, DK), bf16),
            pltpu.VMEM((tok, width), bf16),
            pltpu.VMEM((tok, KEY), bf16),
            pltpu.VMEM((tok, VAL), bf16),
            pltpu.VMEM((tok, VAL), bf16),
            pltpu.VMEM((tok, KEY), bf16),
            pltpu.VMEM((tok, KEY), bf16),
            pltpu.VMEM((tok, KEY), bf16),
            pltpu.VMEM((2, tok, KEY), bf16),
            pltpu.VMEM((5, tok, KEY), f32),
            pltpu.VMEM((1, KEY), f32),
            pltpu.VMEM((2, HEADS, DV, DK), f32),
            pltpu.VMEM((2, HEADS, SPLIT, DVS, DK), bf16),
            pltpu.VMEM((2, HEADS, SPLIT, DVS, DK), bf16),
            pltpu.VMEM((HEADS, tok, DV), f32),
            dma((HEADS + 3,)),
            dma((HEADS,)),
            dma((HEADS, chips)),
            dma((HEADS, chips)),
            dma((HEADS, chips)),
            dma((HEADS, chips)),
            dma((2, HEADS, SPLIT)),
            dma((2, HEADS, SPLIT)),
            dma((HEADS, 2)),
            dma((HEADS, 2)),
        ],
        compiler_params=pltpu.CompilerParams(
            collective_id=0, has_side_effects=True, vmem_limit_bytes=62 * 1024 * 1024),
    )(
        hidden.reshape(tok, width), queries.reshape(tok, KEY), values.reshape(tok, VAL),
        key_weight, decay_down.T, decay_up, decay_bias.reshape(1, KEY),
        span_shift.reshape(1, tok), norm_gain.reshape(1, VAL),
    )
    return result.reshape(seqs, length, VAL)


def solution(mesh):
    in_specs = (
        P("dp", "sp", None), P("dp", "sp", None), P("dp", "sp", None), P("dp", None),
        P(), P(), P(), P("dp", "sp"), P(),
    )
    return jax.shard_map(
        functools.partial(body, mesh.shape["sp"], mesh.shape["dp"]),
        mesh=mesh, in_specs=in_specs, out_specs=P("dp", "sp", None), check_vma=False)
```

profile of v0, /device:TPU:0, one launch (start us, length us, event | category | flops | bytes accessed | tf_op | source)
XLA Modules:
  0.0 59.5 jit_solution(8158445587267491629)
XLA Ops:
  0.0 57.6 %shard_map.91 = bf16[128,2048]{1,0:T(8,128)(2,1)} custom-call(bf16[128,2048]{1,0:T(8,128)(2,1)} %bitcast.8, bf16[128,1024]{1,0:T(8,128)(2,1)} %bitcast.10, bf16[128,2048]{1,0:T(8,128)(2,1)} %bitcast.9, bf16[256,1024]{1,0:T(8,128)(2,1)} %kw.1, bf16[16,2048]{1,0:T(8,128)(2,1)} %bitcast.11, f32[16,1024]{1,0:T(8,128)} %up.1, f32[1,1024]{1,0:T(1,128)} %bitcast.13, ...), custom_call_target="tpu_custom_call" | custom-call | tf_op jit(solution)/shard_map/pallas_call | solution.py:299
  57.6 1.9 %copy.11 = bf16[1,128,2048]{2,1,0:T(8,128)(2,1)} copy(bf16[1,128,2048]{2,1,0:T(8,128)(2,1)} %bitcast.7) | data formatting | bytes 1048576
where the time goes:
time: 59.7 us; the launch traced here: 59.5 us
  Pallas kernels  57.6 us (96%)
  local copies, waits for them, and re-layouts  1.88 us (3%)
    pallas_call x1, Pallas kernels, body(): pl.pallas_call(functools.partial(kernel, n_sp, n_dp), out_shape=jax.Shape...  57.6 us
    unnamed x1, local copies, waits for them, and re-layouts  1.88 us

commit v1 on v0

--- a/solution.py
+++ b/solution.py
@@ -16,6 +16,18 @@
 CORES = 2
 SPLIT = 4
 DVS = DV // SPLIT
+STATES = (0, 1)
+PAIRS = (2, 3)
+PLAN = (
+    ("prep", 0), ("prep", 1), ("prep", 2), ("relay", 0), ("first", 1), ("rest", 1), ("first", 2),
+    ("prep", 3), ("hand", 0), ("forward", 2), ("last", 0), ("wall", 0), ("project", 0), ("values", 1),
+    ("queries", 0), ("queries", 1), ("forward", 3), ("relay", 1), ("rest", 2), ("first", 3),
+    ("hand", 1), ("middle", 0), ("serve", 0), ("last", 1), ("wall", 1), ("project", 1), ("queries", 2),
+    ("queries", 3), ("relay", 2), ("rest", 3), ("hand", 2), ("last", 2), ("middle", 1), ("relay", 3),
+    ("wall", 2), ("project", 2), ("hand", 3), ("serve", 1), ("finish", 0), ("last", 3), ("wall", 3),
+    ("project", 3), ("middle", 2), ("finish", 1), ("middle", 3), ("serve", 2), ("finish", 2),
+    ("serve", 3), ("finish", 3),
+)
 
 decay_tau = 16.0
 norm_eps = 1e-05
@@ -286,6 +298,375 @@
         out_copy(h).wait()
 
 
+def line_kernel(
+    n_sp, n_dp,
+    hid, que, val, kw, down_in, up_in, bias_in, shift_in, gain_in,
+    out,
+    down, up, bias, shift, gain,
+    wbuf, hv, qv, vcat, outv, qf, qb, qx, qs, fac, rate, acc, base,
+    kcat, knear, q2, qraw, ke, vin, kin, sbuf, rbuf, obuf, oin,
+    lsem, osem, wsend, wfirst, wrest, wdiag, wpart, zsend, zrecv,
+):
+    sp = lax.axis_index("sp")
+    dp = lax.axis_index("dp")
+    chip = dp // CORES
+    core = dp % CORES
+    partner = chip * CORES + (1 - core)
+    tok = hv.shape[0]
+    depth = kw.shape[0]
+    half = depth // 2
+    n_chips = n_dp // CORES
+
+    side = sp // 2
+    other = 1 - side
+    mate = sp + 1 - 2 * lax.rem(sp, 2)
+    across = n_sp - 1 - sp
+    edge = (sp == 0) | (sp == n_sp - 1)
+    inner = jnp.logical_not(edge)
+
+    def chip_at(j):
+        return (chip, chip + 1 - 2 * lax.rem(chip, 2), lax.rem(chip + 2, 4), 3 - chip)[j]
+
+    def dev(j):
+        return chip_at(j) * CORES + core
+
+    wlocal = [
+        pltpu.make_async_copy(kw.at[:, pl.ds(h * DK, DK)], wbuf.at[h, dp], lsem.at[h])
+        for h in range(HEADS)
+    ]
+    loads = [
+        pltpu.make_async_copy(a, b, lsem.at[HEADS + i])
+        for i, (a, b) in enumerate((
+            (hid, hv), (que, qv), (val, vcat.at[pl.ds(tok, tok)]),
+            (down_in, down), (up_in, up), (bias_in, bias), (shift_in, shift), (gain_in, gain)))
+    ]
+    barrier = pltpu.get_barrier_semaphore()
+    for j in (1, 2):
+        pl.semaphore_signal(barrier, inc=1, device_id={"dp": dev(j)}, device_id_type=MESH)
+    pl.semaphore_signal(barrier, inc=1, device_id={"dp": partner}, device_id_type=MESH)
+    pl.semaphore_signal(barrier, inc=1, device_id={"sp": mate}, device_id_type=MESH)
+
+    @pl.when(inner)
+    def _():
+        pl.semaphore_signal(barrier, inc=1, device_id={"sp": across}, device_id_type=MESH)
+
+    wlocal[0].start()
+    for i in (2, 0, 3, 4, 5, 6, 1):
+        loads[i].start()
+    for h in range(1, HEADS):
+        wlocal[h].start()
+    loads[7].start()
+    pl.semaphore_wait(barrier, jnp.where(inner, 5, 4))
+
+    def rows(i):
+        return pl.ds(i * half, half)
+
+    def wcopy(h, j, i):
+        part = wbuf.at[h, dp, rows(i)]
+        first = i == j - 1
+        return pltpu.make_async_remote_copy(
+            src_ref=part, dst_ref=part, send_sem=wsend.at[0],
+            recv_sem=wfirst.at[h, i] if first else wrest.at[h],
+            device_id={"dp": dev(j)}, device_id_type=MESH)
+
+    def relay(h, i):
+        part = wbuf.at[h, dev(1 + i), rows(i)]
+        return pltpu.make_async_remote_copy(
+            src_ref=part, dst_ref=part, send_sem=wsend.at[0], recv_sem=wdiag.at[h],
+            device_id={"dp": dev(2 - i)}, device_id_type=MESH)
+
+    def pcopy(h, j):
+        slot = wbuf.at[h, dev(j)]
+        return pltpu.make_async_remote_copy(
+            src_ref=slot, dst_ref=slot, send_sem=wsend.at[0], recv_sem=wpart.at[h],
+            device_id={"dp": partner}, device_id_type=MESH)
+
+    def landed(ref, sem):
+        pltpu.make_async_remote_copy(
+            src_ref=ref, dst_ref=ref, send_sem=zsend.at[0], recv_sem=sem,
+            device_id={"sp": mate}, device_id_type=MESH).wait_recv()
+
+    def gone(ref, sem):
+        pltpu.make_async_remote_copy(
+            src_ref=ref, dst_ref=ref, send_sem=sem, recv_sem=zrecv.at[0],
+            device_id={"sp": mate}, device_id_type=MESH).wait_send()
+
+    def zput(src, dst, send, recv, target):
+        pltpu.make_async_remote_copy(
+            src_ref=src, dst_ref=dst, send_sem=zsend.at[send], recv_sem=zrecv.at[recv],
+            device_id={"sp": target}, device_id_type=MESH).start()
+
+    def wsend_first(h):
+        wlocal[h].wait()
+        for j in (1, 2):
+            wcopy(h, j, j - 1).start()
+        pcopy(h, 0).start()
+
+    def wsend_rest(h):
+        for j in (1, 2):
+            wcopy(h, j, 2 - j).start()
+
+    def wrelay(h):
+        for i in range(2):
+            landed(wbuf.at[h, dev(1 + i), rows(i)], wfirst.at[h, i])
+            relay(h, i).start()
+
+    def wpass(h):
+        landed(wbuf.at[h, 0], wrest.at[h])
+        for j in (1, 2):
+            pcopy(h, j).start()
+
+    def wlast(h):
+        landed(wbuf.at[h, dev(3)], wdiag.at[h])
+        pcopy(h, 3).start()
+
+    def wall(h):
+        landed(wbuf.at[h, pl.ds(0, n_chips)], wpart.at[h])
+
+    VE, QE, KE = 0, HEADS, 2 * HEADS
+    ST = 3 * HEADS
+    VIN = ST + len(STATES) * SPLIT
+    KIN = VIN + 2 * len(PAIRS)
+
+    lo, hi = pl.ds(0, tok), pl.ds(tok, tok)
+
+    def kcols(h):
+        return pl.ds(h * DK, DK)
+
+    def vcols(h):
+        return pl.ds(h * DV, DV)
+
+    def edge_values(h):
+        @pl.when(edge)
+        def _():
+            zput(vcat.at[hi, vcols(h)], vcat.at[lo, vcols(h)], 0, VE + h, mate)
+
+    def inner_values(h):
+        @pl.when(inner)
+        def _():
+            zput(vcat.at[hi, vcols(h)], vin.at[PAIRS.index(h), lo], 0, VIN + 2 * PAIRS.index(h), across)
+
+    def vforward(h):
+        @pl.when(inner)
+        def _():
+            i = PAIRS.index(h)
+            landed(vcat.at[lo, vcols(h)], zrecv.at[VE + h])
+            zput(vcat.at[lo, vcols(h)], vin.at[i, hi], 0, VIN + 2 * i + 1, across)
+
+    def edge_queries(h):
+        @pl.when(edge)
+        def _():
+            zput(qs.at[other, h], qraw.at[h], 1, QE + h, mate)
+
+    wsend_first(0)
+    wsend_rest(0)
+    loads[2].wait()
+    for h in PAIRS:
+        inner_values(h)
+    for h in PAIRS + STATES[:1]:
+        edge_values(h)
+
+    for i in (0, 3):
+        loads[i].wait()
+    low = dot_nt(hv[...], down[...]).astype(bf16).astype(f32)
+    for i in (4, 5, 6, 1):
+        loads[i].wait()
+    steps = shift[...].astype(f32)
+    row = lax.broadcasted_iota(jnp.int32, (tok, DK), 0)
+    first = row < BLOCK
+    ti = lax.broadcasted_iota(jnp.int32, (tok, tok), 0)
+    tj = lax.broadcasted_iota(jnp.int32, (tok, tok), 1)
+    same = (ti < BLOCK) == (tj < BLOCK)
+    below = tj <= ti
+    tri = jnp.where(same & below, 1.0, 0.0).astype(f32)
+
+    def prep(h):
+        cols = kcols(h)
+        pre = jnp.dot(low, up[:, cols], precision=highest, preferred_element_type=f32)
+        pre = pre + bias[:, cols] + jnp.where(first, steps[:, :1], steps[:, BLOCK:BLOCK + 1])
+        logd = (jnp.minimum(pre, 0.0) - jnp.log1p(jnp.exp(-jnp.abs(pre)))) * (1.0 / decay_tau)
+        incl = jnp.dot(tri, logd, precision=highest, preferred_element_type=f32)
+        excl = incl - logd
+        t0 = incl[BLOCK - 1:BLOCK, :]
+        t1 = incl[tok - 1:tok, :]
+        here = jnp.where(first, t0, t1)
+        after = jnp.where(first, t1, 0.0)
+        before = jnp.where(first, 0.0, t0)
+        scaled = qv[:, cols].astype(f32) * DK ** (-0.5)
+        qf[:, cols] = (scaled * jnp.exp(incl)).astype(bf16)
+        qb[:, cols] = (scaled * jnp.exp(-excl)).astype(bf16)
+        qx[:, cols] = (scaled * jnp.exp(here - excl)).astype(bf16)
+        qs[0, h] = (scaled * jnp.exp(incl + before)).astype(bf16)
+        qs[1, h] = (scaled * jnp.exp(here - excl + after)).astype(bf16)
+        fac[0, :, cols] = jnp.exp(-incl)
+        fac[1, :, cols] = jnp.exp(excl)
+        fac[2, :, cols] = jnp.exp(here - incl)
+        fac[3, :, cols] = jnp.exp(here - incl + after)
+        fac[4, :, cols] = jnp.exp(excl + before)
+        rate[:, cols] = jnp.exp(t0 + t1)
+
+    def project(h):
+        cols = kcols(h)
+        weights = wbuf[h].reshape(n_dp * depth, DK)
+        keys = jnp.dot(hv[...], weights, preferred_element_type=f32).astype(bf16).astype(f32)
+        kcat[h, hi] = (keys * fac[3 + side, :, cols]).astype(bf16)
+
+        @pl.when(edge)
+        def _():
+            zput(kcat.at[h, hi], ke.at[h], 2, KE + h, mate)
+
+        if h in PAIRS:
+            @pl.when(inner)
+            def _():
+                i = PAIRS.index(h)
+                zput(kcat.at[h, hi], kin.at[i, lo], 1, KIN + 2 * i, across)
+
+        knear[h] = (keys * fac[3 + other, :, cols]).astype(bf16)
+        v = vcat[hi, vcols(h)]
+        kf = (keys * fac[0, :, cols]).astype(bf16)
+        kb = (keys * fac[1, :, cols]).astype(bf16)
+        kx = (keys * fac[2, :, cols]).astype(bf16)
+        query_f, query_b, query_x = qf[:, cols], qb[:, cols], qx[:, cols]
+        lower = jnp.where(same, dot_nt(query_f, kf), dot_nt(query_f, kx))
+        upper = jnp.where(same, dot_nt(query_b, kb), dot_nt(query_x, kb))
+        scores = jnp.where(below, lower, upper).astype(bf16)
+        acc[h] = jnp.dot(scores, v, preferred_element_type=f32)
+
+    def piece(h, s):
+        return pl.ds(h * DV + s * DVS, DVS)
+
+    def middle(h):
+        @pl.when(inner)
+        def _():
+            if h in STATES:
+                landed(vcat.at[lo, vcols(h)], zrecv.at[VE + h])
+            landed(ke.at[h], zrecv.at[KE + h])
+            far_keys = ke[h]
+            kcat[h, lo] = (far_keys.astype(f32) * rate[:, kcols(h)]).astype(bf16)
+            if h in PAIRS:
+                i = PAIRS.index(h)
+                zput(kcat.at[h, lo], kin.at[i, hi], 1, KIN + 2 * i + 1, across)
+            else:
+                i = STATES.index(h)
+                both = kcat[h]
+                for s in range(SPLIT):
+                    sbuf[i, s] = dot_tn(vcat[:, piece(h, s)], both).astype(bf16)
+                    zput(sbuf.at[i, s], rbuf.at[i, s], 2, ST + i * SPLIT + s, across)
+            seen = dot_nt(qs[side, h], far_keys).astype(bf16)
+            acc[h] += jnp.dot(seen, vcat[lo, vcols(h)], preferred_element_type=f32)
+
+    def serve(h):
+        @pl.when(inner)
+        def _():
+            landed(qraw.at[h], zrecv.at[QE + h])
+            raw = qraw[h]
+            q2[h, lo] = qs[other, h]
+            q2[h, hi] = (raw.astype(f32) * rate[:, kcols(h)]).astype(bf16)
+            near = dot_nt(raw, knear[h]).astype(bf16)
+            base[h] = jnp.dot(near, vcat[hi, vcols(h)], preferred_element_type=f32)
+
+    def emit(h):
+        cols = vcols(h)
+        mixed = acc[h].astype(bf16).astype(f32)
+        scale = lax.rsqrt(jnp.mean(mixed * mixed, axis=-1, keepdims=True) + norm_eps)
+        outv[:, cols] = (mixed * scale * gain[:, cols]).astype(bf16)
+        pltpu.make_async_copy(outv.at[:, cols], out.at[:, cols], osem.at[0]).start()
+
+    def finish(h):
+        @pl.when(inner)
+        def _():
+            if h in PAIRS:
+                i = PAIRS.index(h)
+                for part, where in enumerate((lo, hi)):
+                    landed(vin.at[i, where], zrecv.at[VIN + 2 * i + part])
+                    landed(kin.at[i, where], zrecv.at[KIN + 2 * i + part])
+                seen = dot_nt(q2[h], kin[i]).astype(bf16)
+            for s in range(SPLIT):
+                cut = pl.ds(s * DVS, DVS)
+                if h in PAIRS:
+                    both = jnp.dot(seen, vin[i, :, cut], preferred_element_type=f32)
+                else:
+                    i = STATES.index(h)
+                    landed(rbuf.at[i, s], zrecv.at[ST + i * SPLIT + s])
+                    both = dot_nt(q2[h], rbuf[i, s])
+                obuf[h, s] = (base[h, :, cut] + both[tok:]).astype(bf16)
+                zput(obuf.at[h, s], oin.at[h, s], 3, h * SPLIT + s, mate)
+                acc[h, :, cut] += both[:tok]
+
+        @pl.when(edge)
+        def _():
+            for s in range(SPLIT):
+                landed(oin.at[h, s], zrecv.at[h * SPLIT + s])
+                acc[h, :, pl.ds(s * DVS, DVS)] += oin[h, s].astype(f32)
+
+        emit(h)
+
+    names = dict(
+        prep=prep, first=wsend_first, rest=wsend_rest, relay=wrelay, hand=wpass, last=wlast, wall=wall,
+        project=project, middle=middle, serve=serve, finish=finish, values=edge_values,
+        queries=edge_queries, forward=vforward)
+    loads[7].wait()
+    for name, h in PLAN:
+        names[name](h)
+
+    gone(wbuf.at[:, pl.ds(0, n_dp - 1)], wsend.at[0])
+
+    @pl.when(edge)
+    def _():
+        gone(vcat.at[hi], zsend.at[0])
+        gone(qraw, zsend.at[1])
+        gone(ke, zsend.at[2])
+
+    @pl.when(inner)
+    def _():
+        gone(vin, zsend.at[0])
+        gone(kin, zsend.at[1])
+        gone(sbuf, zsend.at[2])
+        gone(obuf, zsend.at[3])
+
+    pltpu.make_async_copy(outv, out, osem.at[0]).wait()
+
+
+def line_scratch(n_dp, tok, width, depth, rank):
+    dma = pltpu.SemaphoreType.DMA
+    v = pltpu.VMEM
+    pairs, states = len(PAIRS), len(STATES)
+    return [
+        v((rank, width), bf16), v((rank, KEY), f32), v((1, KEY), f32), v((1, tok), bf16), v((1, VAL), f32),
+        v((HEADS, n_dp, depth, DK), bf16),
+        v((tok, width), bf16),
+        v((tok, KEY), bf16),
+        v((2 * tok, VAL), bf16),
+        v((tok, VAL), bf16),
+        v((tok, KEY), bf16), v((tok, KEY), bf16), v((tok, KEY), bf16),
+        v((2, HEADS, tok, DK), bf16),
+        v((5, tok, KEY), f32),
+        v((1, KEY), f32),
+        v((HEADS, tok, DV), f32),
+        v((HEADS, tok, DV), f32),
+        v((HEADS, 2 * tok, DK), bf16),
+        v((HEADS, tok, DK), bf16),
+        v((HEADS, 2 * tok, DK), bf16),
+        v((HEADS, tok, DK), bf16),
+        v((HEADS, tok, DK), bf16),
+        v((pairs, 2 * tok, DV), bf16),
+        v((pairs, 2 * tok, DK), bf16),
+        v((states, SPLIT, DVS, DK), bf16),
+        v((states, SPLIT, DVS, DK), bf16),
+        v((HEADS, SPLIT, tok, DVS), bf16),
+        v((HEADS, SPLIT, tok, DVS), bf16),
+        dma((HEADS + 8,)),
+        dma((1,)),
+        dma((1,)),
+        dma((HEADS, 2)),
+        dma((HEADS,)),
+        dma((HEADS,)),
+        dma((HEADS,)),
+        dma((4,)),
+        dma((3 * HEADS + states * SPLIT + 4 * pairs,)),
+    ]
+
+
 def body(n_sp, n_dp, hidden, queries, values, key_weight, decay_down, decay_up, decay_bias,
          span_shift, norm_gain):
     seqs, length, width = hidden.shape
@@ -294,6 +675,22 @@
     chips = n_dp // CORES
     depth = key_weight.shape[0]
     anywhere = pl.BlockSpec(memory_space=pl.ANY)
+    operands = (
+        hidden.reshape(tok, width), queries.reshape(tok, KEY), values.reshape(tok, VAL),
+        key_weight, decay_down.T, decay_up, decay_bias.reshape(1, KEY),
+        span_shift.reshape(1, tok), norm_gain.reshape(1, VAL),
+    )
+    if n_sp == 4 and chips == 4:
+        result = pl.pallas_call(
+            functools.partial(line_kernel, n_sp, n_dp),
+            out_shape=jax.ShapeDtypeStruct((tok, VAL), bf16),
+            in_specs=[anywhere] * 9,
+            out_specs=anywhere,
+            scratch_shapes=line_scratch(n_dp, tok, width, depth, decay_up.shape[0]),
+            compiler_params=pltpu.CompilerParams(
+                collective_id=0, has_side_effects=True, vmem_limit_bytes=62 * 1024 * 1024),
+        )(*operands)
+        return result.reshape(seqs, length, VAL)
     vmem = pl.BlockSpec(memory_space=pltpu.VMEM)
     dma = pltpu.SemaphoreType.DMA
     result = pl.pallas_call(
@@ -330,11 +727,7 @@
         ],
         compiler_params=pltpu.CompilerParams(
             collective_id=0, has_side_effects=True, vmem_limit_bytes=62 * 1024 * 1024),
-    )(
-        hidden.reshape(tok, width), queries.reshape(tok, KEY), values.reshape(tok, VAL),
-        key_weight, decay_down.T, decay_up, decay_bias.reshape(1, KEY),
-        span_shift.reshape(1, tok), norm_gain.reshape(1, VAL),
-    )
+    )(*operands)
     return result.reshape(seqs, length, VAL)
 
 

time: 59.7 us -> 51.1 us (0.86)
  Pallas kernels: 57.6 us -> 49.1 us
    pallas_call x1, Pallas kernels: 57.6 us -> 49.1 us  [body(): pl.pallas_call(functools.partial(line_kernel, n_sp, n_dp), out_shape=jax....]
where the time goes in v1:
time: 51.1 us; the launch traced here: 50.9 us
  Pallas kernels  49.1 us (96%)
  local copies, waits for them, and re-layouts  1.88 us (4%)
    pallas_call x1, Pallas kernels, body(): pl.pallas_call(functools.partial(line_kernel, n_sp, n_dp), out_shape=jax....  49.1 us
    unnamed x1, local copies, waits for them, and re-layouts  1.88 us

profile of v1, /device:TPU:0, one launch (start us, length us, event | category | flops | bytes accessed | tf_op | source)
XLA Modules:
  0.0 50.9 jit_solution(9009814498571507754)
XLA Ops:
  0.0 49.1 %shard_map.91 = bf16[128,2048]{1,0:T(8,128)(2,1)} custom-call(bf16[128,2048]{1,0:T(8,128)(2,1)} %bitcast.8, bf16[128,1024]{1,0:T(8,128)(2,1)} %bitcast.10, bf16[128,2048]{1,0:T(8,128)(2,1)} %bitcast.9, bf16[256,1024]{1,0:T(8,128)(2,1)} %kw.1, bf16[16,2048]{1,0:T(8,128)(2,1)} %bitcast.11, f32[16,1024]{1,0:T(8,128)} %up_in.1, f32[1,1024]{1,0:T(1,128)} %bitcast.13, ...), custom_call_target="tpu_custom_call" | custom-call | tf_op jit(solution)/shard_map/pallas_call | solution.py:684
  49.1 1.9 %copy.11 = bf16[1,128,2048]{2,1,0:T(8,128)(2,1)} copy(bf16[1,128,2048]{2,1,0:T(8,128)(2,1)} %bitcast.7) | data formatting | bytes 1048576

commit v2 on v1

--- a/solution.py
+++ b/solution.py
@@ -18,15 +18,27 @@
 DVS = DV // SPLIT
 STATES = (0, 1)
 PAIRS = (2, 3)
-PLAN = (
+EDGE_PLAN = (
     ("prep", 0), ("prep", 1), ("prep", 2), ("relay", 0), ("first", 1), ("rest", 1), ("first", 2),
-    ("prep", 3), ("hand", 0), ("forward", 2), ("last", 0), ("wall", 0), ("project", 0), ("values", 1),
-    ("queries", 0), ("queries", 1), ("forward", 3), ("relay", 1), ("rest", 2), ("first", 3),
-    ("hand", 1), ("middle", 0), ("serve", 0), ("last", 1), ("wall", 1), ("project", 1), ("queries", 2),
-    ("queries", 3), ("relay", 2), ("rest", 3), ("hand", 2), ("last", 2), ("middle", 1), ("relay", 3),
-    ("wall", 2), ("project", 2), ("hand", 3), ("serve", 1), ("finish", 0), ("last", 3), ("wall", 3),
-    ("project", 3), ("middle", 2), ("finish", 1), ("middle", 3), ("serve", 2), ("finish", 2),
-    ("serve", 3), ("finish", 3),
+    ("prep", 3), ("hand", 0), ("last", 0), ("wall", 0), ("project", 0), ("values", 1), ("queries", 0),
+    ("relay", 1), ("rest", 2), ("first", 3), ("score", 0), ("hand", 1),
+    ("relay", 2), ("rest", 3), ("last", 1), ("wall", 1), ("project", 1), ("queries", 1), ("queries", 2),
+    ("hand", 2), ("score", 1), ("relay", 3), ("last", 2), ("wall", 2), ("project", 2), ("queries", 3),
+    ("hand", 3), ("score", 2), ("last", 3), ("wall", 3), ("project", 3), ("score", 3),
+    ("finish", 0), ("finish", 2), ("finish", 3), ("finish", 1),
+)
+INNER_PLAN = (
+    ("prep", 0), ("prep", 1), ("prep", 2), ("relay", 0), ("first", 1), ("rest", 1), ("first", 2),
+    ("prep", 3), ("hand", 0), ("forward", 2), ("last", 0), ("forward", 3), ("wall", 0), ("project", 0),
+    ("relay", 1), ("rest", 2), ("first", 3), ("score", 0), ("hand", 1),
+    ("relay", 2), ("rest", 3), ("middle", 0), ("push", 0, 0), ("push", 0, 1), ("push", 0, 2), ("push", 0, 3), ("cross", 0),
+    ("last", 1), ("hand", 2), ("wall", 1), ("project", 1), ("score", 1),
+    ("relay", 3), ("last", 2), ("middle", 1), ("push", 1, 0), ("push", 1, 1), ("cross", 1),
+    ("serve", 0), ("wall", 2), ("project", 2), ("score", 2), ("hand", 3), ("last", 3),
+    ("take", 0, 0), ("take", 0, 1), ("serve", 1), ("wall", 3), ("project", 3), ("middle", 2), ("score", 3), ("cross", 2),
+    ("take", 0, 2), ("take", 0, 3), ("emit", 0), ("middle", 3), ("push", 1, 2), ("push", 1, 3), ("cross", 3),
+    ("take", 1, 0), ("take", 1, 1),
+    ("serve", 2), ("serve", 3), ("pair", 2), ("emit", 2), ("pair", 3), ("emit", 3), ("take", 1, 2), ("take", 1, 3), ("emit", 1),
 )
 
 decay_tau = 16.0
@@ -303,7 +315,7 @@
     hid, que, val, kw, down_in, up_in, bias_in, shift_in, gain_in,
     out,
     down, up, bias, shift, gain,
-    wbuf, hv, qv, vcat, outv, qf, qb, qx, qs, fac, rate, acc, base,
+    wbuf, hv, qv, vcat, outv, own, qf, qb, qx, qs, fac, rate, acc, base,
     kcat, knear, q2, qraw, ke, vin, kin, sbuf, rbuf, obuf, oin,
     lsem, osem, wsend, wfirst, wrest, wdiag, wpart, zsend, zrecv,
 ):
@@ -437,34 +449,32 @@
         return pl.ds(h * DV, DV)
 
     def edge_values(h):
-        @pl.when(edge)
-        def _():
-            zput(vcat.at[hi, vcols(h)], vcat.at[lo, vcols(h)], 0, VE + h, mate)
+        zput(vcat.at[hi, vcols(h)], vcat.at[lo, vcols(h)], 0, VE + h, mate)
 
     def inner_values(h):
-        @pl.when(inner)
-        def _():
-            zput(vcat.at[hi, vcols(h)], vin.at[PAIRS.index(h), lo], 0, VIN + 2 * PAIRS.index(h), across)
+        zput(vcat.at[hi, vcols(h)], vin.at[PAIRS.index(h), lo], 0, VIN + 2 * PAIRS.index(h), across)
 
     def vforward(h):
-        @pl.when(inner)
-        def _():
-            i = PAIRS.index(h)
-            landed(vcat.at[lo, vcols(h)], zrecv.at[VE + h])
-            zput(vcat.at[lo, vcols(h)], vin.at[i, hi], 0, VIN + 2 * i + 1, across)
+        i = PAIRS.index(h)
+        landed(vcat.at[lo, vcols(h)], zrecv.at[VE + h])
+        zput(vcat.at[lo, vcols(h)], vin.at[i, hi], 0, VIN + 2 * i + 1, across)
 
     def edge_queries(h):
-        @pl.when(edge)
-        def _():
-            zput(qs.at[other, h], qraw.at[h], 1, QE + h, mate)
+        zput(qs.at[other, h], qraw.at[h], 1, QE + h, mate)
 
     wsend_first(0)
     wsend_rest(0)
     loads[2].wait()
-    for h in PAIRS:
-        inner_values(h)
-    for h in PAIRS + STATES[:1]:
-        edge_values(h)
+
+    @pl.when(inner)
+    def _():
+        for h in PAIRS:
+            inner_values(h)
+
+    @pl.when(edge)
+    def _():
+        for h in PAIRS + STATES[:1]:
+            edge_values(h)
 
     for i in (0, 3):
         loads[i].wait()
@@ -480,7 +490,7 @@
     below = tj <= ti
     tri = jnp.where(same & below, 1.0, 0.0).astype(f32)
 
-    def prep(h):
+    def prep(at_edge, h):
         cols = kcols(h)
         pre = jnp.dot(low, up[:, cols], precision=highest, preferred_element_type=f32)
         pre = pre + bias[:, cols] + jnp.where(first, steps[:, :1], steps[:, BLOCK:BLOCK + 1])
@@ -496,32 +506,41 @@
         qf[:, cols] = (scaled * jnp.exp(incl)).astype(bf16)
         qb[:, cols] = (scaled * jnp.exp(-excl)).astype(bf16)
         qx[:, cols] = (scaled * jnp.exp(here - excl)).astype(bf16)
-        qs[0, h] = (scaled * jnp.exp(incl + before)).astype(bf16)
-        qs[1, h] = (scaled * jnp.exp(here - excl + after)).astype(bf16)
+        ahead, behind = incl + before, here - excl + after
+        if at_edge:
+            qs[other, h] = (scaled * jnp.exp(jnp.where(side == 1, ahead, behind))).astype(bf16)
+        else:
+            qs[0, h] = (scaled * jnp.exp(ahead)).astype(bf16)
+            qs[1, h] = (scaled * jnp.exp(behind)).astype(bf16)
         fac[0, :, cols] = jnp.exp(-incl)
         fac[1, :, cols] = jnp.exp(excl)
         fac[2, :, cols] = jnp.exp(here - incl)
-        fac[3, :, cols] = jnp.exp(here - incl + after)
-        fac[4, :, cols] = jnp.exp(excl + before)
-        rate[:, cols] = jnp.exp(t0 + t1)
-
-    def project(h):
+        ahead, behind = here - incl + after, excl + before
+        if at_edge:
+            fac[3 + side, :, cols] = jnp.exp(jnp.where(side == 0, ahead, behind))
+        else:
+            fac[3, :, cols] = jnp.exp(ahead)
+            fac[4, :, cols] = jnp.exp(behind)
+            rate[:, cols] = jnp.exp(t0 + t1)
+
+    def project(at_edge, h):
         cols = kcols(h)
         weights = wbuf[h].reshape(n_dp * depth, DK)
-        keys = jnp.dot(hv[...], weights, preferred_element_type=f32).astype(bf16).astype(f32)
+        keys = jnp.dot(hv[...], weights, preferred_element_type=f32).astype(bf16)
+        own[:, cols] = keys
+        keys = keys.astype(f32)
         kcat[h, hi] = (keys * fac[3 + side, :, cols]).astype(bf16)
-
-        @pl.when(edge)
-        def _():
+        if at_edge:
             zput(kcat.at[h, hi], ke.at[h], 2, KE + h, mate)
-
-        if h in PAIRS:
-            @pl.when(inner)
-            def _():
-                i = PAIRS.index(h)
-                zput(kcat.at[h, hi], kin.at[i, lo], 1, KIN + 2 * i, across)
-
-        knear[h] = (keys * fac[3 + other, :, cols]).astype(bf16)
+        elif h in PAIRS:
+            i = PAIRS.index(h)
+            zput(kcat.at[h, hi], kin.at[i, lo], 1, KIN + 2 * i, across)
+
+    def score(at_edge, h):
+        cols = kcols(h)
+        keys = own[:, cols].astype(f32)
+        if not at_edge:
+            knear[h] = (keys * fac[3 + other, :, cols]).astype(bf16)
         v = vcat[hi, vcols(h)]
         kf = (keys * fac[0, :, cols]).astype(bf16)
         kb = (keys * fac[1, :, cols]).astype(bf16)
@@ -536,34 +555,35 @@
         return pl.ds(h * DV + s * DVS, DVS)
 
     def middle(h):
-        @pl.when(inner)
-        def _():
-            if h in STATES:
-                landed(vcat.at[lo, vcols(h)], zrecv.at[VE + h])
-            landed(ke.at[h], zrecv.at[KE + h])
-            far_keys = ke[h]
-            kcat[h, lo] = (far_keys.astype(f32) * rate[:, kcols(h)]).astype(bf16)
-            if h in PAIRS:
-                i = PAIRS.index(h)
-                zput(kcat.at[h, lo], kin.at[i, hi], 1, KIN + 2 * i + 1, across)
-            else:
-                i = STATES.index(h)
-                both = kcat[h]
-                for s in range(SPLIT):
-                    sbuf[i, s] = dot_tn(vcat[:, piece(h, s)], both).astype(bf16)
-                    zput(sbuf.at[i, s], rbuf.at[i, s], 2, ST + i * SPLIT + s, across)
-            seen = dot_nt(qs[side, h], far_keys).astype(bf16)
-            acc[h] += jnp.dot(seen, vcat[lo, vcols(h)], preferred_element_type=f32)
+        if h in STATES:
+            landed(vcat.at[lo, vcols(h)], zrecv.at[VE + h])
+        landed(ke.at[h], zrecv.at[KE + h])
+        far_keys = ke[h]
+        kcat[h, lo] = (far_keys.astype(f32) * rate[:, kcols(h)]).astype(bf16)
+        if h in PAIRS:
+            i = PAIRS.index(h)
+            zput(kcat.at[h, lo], kin.at[i, hi], 1, KIN + 2 * i + 1, across)
+        else:
+            i = STATES.index(h)
+            both = kcat[h]
+            for s in range(SPLIT):
+                sbuf[i, s] = dot_tn(vcat[:, piece(h, s)], both).astype(bf16)
+
+    def push(h, s):
+        i = STATES.index(h)
+        zput(sbuf.at[i, s], rbuf.at[i, s], 2, ST + i * SPLIT + s, across)
+
+    def cross(h):
+        seen = dot_nt(qs[side, h], ke[h]).astype(bf16)
+        acc[h] += jnp.dot(seen, vcat[lo, vcols(h)], preferred_element_type=f32)
 
     def serve(h):
-        @pl.when(inner)
-        def _():
-            landed(qraw.at[h], zrecv.at[QE + h])
-            raw = qraw[h]
-            q2[h, lo] = qs[other, h]
-            q2[h, hi] = (raw.astype(f32) * rate[:, kcols(h)]).astype(bf16)
-            near = dot_nt(raw, knear[h]).astype(bf16)
-            base[h] = jnp.dot(near, vcat[hi, vcols(h)], preferred_element_type=f32)
+        landed(qraw.at[h], zrecv.at[QE + h])
+        raw = qraw[h]
+        q2[h, lo] = qs[other, h]
+        q2[h, hi] = (raw.astype(f32) * rate[:, kcols(h)]).astype(bf16)
+        near = dot_nt(raw, knear[h]).astype(bf16)
+        base[h] = jnp.dot(near, vcat[hi, vcols(h)], preferred_element_type=f32)
 
     def emit(h):
         cols = vcols(h)
@@ -572,42 +592,51 @@
         outv[:, cols] = (mixed * scale * gain[:, cols]).astype(bf16)
         pltpu.make_async_copy(outv.at[:, cols], out.at[:, cols], osem.at[0]).start()
 
+    def share(h, s, both):
+        cut = pl.ds(s * DVS, DVS)
+        obuf[h, s] = (base[h, :, cut] + both[tok:]).astype(bf16)
+        zput(obuf.at[h, s], oin.at[h, s], 3, h * SPLIT + s, mate)
+        acc[h, :, cut] += both[:tok]
+
+    def take(h, s):
+        i = STATES.index(h)
+        landed(rbuf.at[i, s], zrecv.at[ST + i * SPLIT + s])
+        share(h, s, dot_nt(q2[h], rbuf[i, s]))
+
+    def pair(h):
+        i = PAIRS.index(h)
+        for part, where in enumerate((lo, hi)):
+            landed(vin.at[i, where], zrecv.at[VIN + 2 * i + part])
+            landed(kin.at[i, where], zrecv.at[KIN + 2 * i + part])
+        seen = dot_nt(q2[h], kin[i]).astype(bf16)
+        for s in range(SPLIT):
+            share(h, s, jnp.dot(seen, vin[i, :, pl.ds(s * DVS, DVS)], preferred_element_type=f32))
+
     def finish(h):
-        @pl.when(inner)
-        def _():
-            if h in PAIRS:
-                i = PAIRS.index(h)
-                for part, where in enumerate((lo, hi)):
-                    landed(vin.at[i, where], zrecv.at[VIN + 2 * i + part])
-                    landed(kin.at[i, where], zrecv.at[KIN + 2 * i + part])
-                seen = dot_nt(q2[h], kin[i]).astype(bf16)
-            for s in range(SPLIT):
-                cut = pl.ds(s * DVS, DVS)
-                if h in PAIRS:
-                    both = jnp.dot(seen, vin[i, :, cut], preferred_element_type=f32)
-                else:
-                    i = STATES.index(h)
-                    landed(rbuf.at[i, s], zrecv.at[ST + i * SPLIT + s])
-                    both = dot_nt(q2[h], rbuf[i, s])
-                obuf[h, s] = (base[h, :, cut] + both[tok:]).astype(bf16)
-                zput(obuf.at[h, s], oin.at[h, s], 3, h * SPLIT + s, mate)
-                acc[h, :, cut] += both[:tok]
-
-        @pl.when(edge)
-        def _():
-            for s in range(SPLIT):
-                landed(oin.at[h, s], zrecv.at[h * SPLIT + s])
-                acc[h, :, pl.ds(s * DVS, DVS)] += oin[h, s].astype(f32)
-
+        for s in range(SPLIT):
+            landed(oin.at[h, s], zrecv.at[h * SPLIT + s])
+            acc[h, :, pl.ds(s * DVS, DVS)] += oin[h, s].astype(f32)
         emit(h)
 
-    names = dict(
-        prep=prep, first=wsend_first, rest=wsend_rest, relay=wrelay, hand=wpass, last=wlast, wall=wall,
-        project=project, middle=middle, serve=serve, finish=finish, values=edge_values,
-        queries=edge_queries, forward=vforward)
     loads[7].wait()
-    for name, h in PLAN:
-        names[name](h)
+
+    def run(at_edge, plan):
+        names = dict(
+            prep=functools.partial(prep, at_edge), first=wsend_first, rest=wsend_rest, relay=wrelay,
+            hand=wpass, last=wlast, wall=wall, project=functools.partial(project, at_edge),
+            score=functools.partial(score, at_edge), middle=middle, serve=serve,
+            push=push, cross=cross, take=take, pair=pair, emit=emit, finish=finish, values=edge_values, queries=edge_queries,
+            forward=vforward)
+        for name, *where in plan:
+            names[name](*where)
+
+    @pl.when(edge)
+    def _():
+        run(True, EDGE_PLAN)
+
+    @pl.when(inner)
+    def _():
+        run(False, INNER_PLAN)
 
     gone(wbuf.at[:, pl.ds(0, n_dp - 1)], wsend.at[0])
 
@@ -638,7 +667,7 @@
         v((tok, KEY), bf16),
         v((2 * tok, VAL), bf16),
         v((tok, VAL), bf16),
-        v((tok, KEY), bf16), v((tok, KEY), bf16), v((tok, KEY), bf16),
+        v((tok, KEY), bf16), v((tok, KEY), bf16), v((tok, KEY), bf16), v((tok, KEY), bf16),
         v((2, HEADS, tok, DK), bf16),
         v((5, tok, KEY), f32),
         v((1, KEY), f32),

time: 51.1 us -> 44.4 us (0.87)
  Pallas kernels: 49.1 us -> 42.4 us
    pallas_call x1, Pallas kernels: 49.1 us -> 42.4 us  [body(): pl.pallas_call(functools.partial(line_kernel, n_sp, n_dp), out_shape=jax....]
where the time goes in v2:
time: 44.4 us; the launch traced here: 44.3 us
  Pallas kernels  42.4 us (95%)
  local copies, waits for them, and re-layouts  1.88 us (4%)
    pallas_call x1, Pallas kernels, body(): pl.pallas_call(functools.partial(line_kernel, n_sp, n_dp), out_shape=jax....  42.4 us
    unnamed x1, local copies, waits for them, and re-layouts  1.88 us

profile of v2, /device:TPU:0, one launch (start us, length us, event | category | flops | bytes accessed | tf_op | source)
XLA Modules:
  0.0 44.3 jit_solution(17067817728982469099)
XLA Ops:
  0.0 42.4 %shard_map.91 = bf16[128,2048]{1,0:T(8,128)(2,1)} custom-call(bf16[128,2048]{1,0:T(8,128)(2,1)} %bitcast.8, bf16[128,1024]{1,0:T(8,128)(2,1)} %bitcast.10, bf16[128,2048]{1,0:T(8,128)(2,1)} %bitcast.9, bf16[256,1024]{1,0:T(8,128)(2,1)} %kw.1, bf16[16,2048]{1,0:T(8,128)(2,1)} %bitcast.11, f32[16,1024]{1,0:T(8,128)} %up_in.1, f32[1,1024]{1,0:T(1,128)} %bitcast.13, ...), custom_call_target="tpu_custom_call" | custom-call | tf_op jit(solution)/shard_map/pallas_call | solution.py:713
  42.4 1.9 %copy.11 = bf16[1,128,2048]{2,1,0:T(8,128)(2,1)} copy(bf16[1,128,2048]{2,1,0:T(8,128)(2,1)} %bitcast.7) | data formatting | bytes 1048576
